TPU v7x, 32 devices: a whole 2x2x4 slice. The times are simulated.
32 devices in a mesh: fs: 8 (over z, y), tp: 4 (over x, core).
Axes of the slice: x: 2, y: 2, z: 4, core: 2. Of those that a mesh axis runs over, the one named last changes fastest.
Arguments:
- tokens: bfloat16 [4096, 2048], P(('fs', 'tp')), may hold values from -6 to 6
- norm_one: float32 [2048], replicated, may hold values from 0.1 to 1.9
- gate_one: bfloat16 [2048, 4608], P('fs', 'tp'), may hold values from -0.125 to 0.125
- up_one: bfloat16 [2048, 4608], P('fs', 'tp'), may hold values from -0.125 to 0.125
- down_one: bfloat16 [4608, 2048], P('tp', 'fs'), may hold values from -0.1875 to 0.1875
- norm_two: float32 [2048], replicated, may hold values from 0.1 to 1.9
- gate_two: bfloat16 [2048, 4608], P('fs', 'tp'), may hold values from -0.125 to 0.125
- up_two: bfloat16 [2048, 4608], P('fs', 'tp'), may hold values from -0.125 to 0.125
- down_two: bfloat16 [4608, 2048], P('tp', 'fs'), may hold values from -0.1875 to 0.1875
Outputs:
- result: bfloat16 [4096, 2048], P(('fs', 'tp'))
All inputs are finite; a program needn't handle non-finite values.
Results may differ from a plain program's by a relative error of at most 0.015.
Values may be sent and summed in bfloat16 or wider, within the bound.
A program may use at most 64 MiB of HBM per device.

v0:
```python
import jax
import jax.numpy as jnp
from jax import lax
from jax.sharding import PartitionSpec as P

eps = 1e-06


def normalize(rows, gain):
    values = rows.astype(jnp.float32)
    scaled = values * lax.rsqrt(jnp.mean(values * values, axis=-1, keepdims=True) + eps)
    return (scaled * gain).astype(jnp.bfloat16)


def hidden_units(rows, gain, gate_w, up_w):
    normed = normalize(rows, gain)
    gate_full, up_full = (
        lax.all_gather(gate_w, "fs", axis=0, tiled=True),
        lax.all_gather(up_w, "fs", axis=0, tiled=True),
    )
    gate_sum = jnp.dot(normed, gate_full, preferred_element_type=jnp.float32)
    up_sum = jnp.dot(normed, up_full, preferred_element_type=jnp.float32)
    return (jax.nn.silu(gate_sum) * up_sum).astype(jnp.bfloat16)


def down_terms(hidden, down_w):
    return jnp.dot(
        hidden, lax.all_gather(down_w, "fs", axis=1, tiled=True), preferred_element_type=jnp.float32
    )


def on_device(tokens, norm_one, gate_one, up_one, down_one, norm_two, gate_two, up_two, down_two):
    gathered = lax.all_gather(tokens, "tp", axis=0, tiled=True)
    first_terms = down_terms(hidden_units(gathered, norm_one, gate_one, up_one), down_one)
    summed = lax.psum(first_terms.astype(jnp.bfloat16), "tp").astype(jnp.float32)
    mid_group = (gathered.astype(jnp.float32) + 0.5 * summed).astype(jnp.bfloat16)
    mid_rows = lax.dynamic_slice_in_dim(
        mid_group, lax.axis_index("tp") * tokens.shape[0], tokens.shape[0], 0
    )
    second_terms = down_terms(hidden_units(mid_group, norm_two, gate_two, up_two), down_two)
    summed_two = lax.psum_scatter(
        second_terms.astype(jnp.bfloat16), "tp", scatter_dimension=0, tiled=True
    ).astype(jnp.float32)
    return (mid_rows.astype(jnp.float32) + 0.5 * summed_two).astype(jnp.bfloat16)


def solution(mesh):
    return jax.shard_map(
        on_device,
        mesh=mesh,
        in_specs=(
            P(("fs", "tp"), None),
            P(),
            P("fs", "tp"),
            P("fs", "tp"),
            P("tp", "fs"),
            P(),
            P("fs", "tp"),
            P("fs", "tp"),
            P("tp", "fs"),
        ),
        out_specs=P(("fs", "tp"), None),
        check_vma=False,
    )
```

profile of v0, /device:TPU:0, one launch (start us, length us, event | category | flops | bytes accessed | tf_op | source)
XLA Modules:
  0.0 631.1 jit_solution(18163117887727268943)
XLA Ops:
  6.5 0.0 copy-start.2
  6.5 0.0 all-gather.8.cloned.1.call-start
  6.5 0.7 all-gather.8.cloned.1.call-update
  7.3 0.0 all-gather.10.cloned.1.call-start
  7.3 0.7 all-gather.10.cloned.1.call-update
  8.0 0.0 all-gather.12.cloned.1.call-start
  8.1 0.7 all-gather.12.cloned.1.call-update
  8.7 0.0 all-gather.14.cloned.1.call-start
  8.8 0.5 all-gather.14.cloned.1.call-update
  9.3 0.0 all-reduce.2.cloned.1.call-start
  9.4 24.8 %all-gather.8.cloned.1.call-done = bf16[512,2048]{1,0:T(8,128)(2,1)} async-done(((bf16[128,2048]{1,0:T(8,128)(2,1)}), bf16[512,2048]{1,0:T(8,128)(2,1)}) %all-gather.8.cloned.1.call-update) | async-done | bytes 2097168 | tf_op jit(solution)/shard_map/all_gather | solution.py:33
  34.2 2.1 fusion.3
  36.3 0.0 copy-start
  36.3 79.5 %all-gather.10.cloned.1.call-done = bf16[2048,1152]{1,0:T(8,128)(2,1)} async-done(((bf16[256,1152]{1,0:T(8,128)(2,1)}), bf16[2048,1152]{1,0:T(8,128)(2,1)}) %all-gather.10.cloned.1.call-update) | async-done | bytes 4718608 | tf_op jit(solution)/shard_map/all_gather | solution.py:18
  115.8 0.0 copy-done.2
  115.8 7.3 %fusion.11 = f32[512,1152]{1,0:T(8,128)} fusion(bf16[2048,1152]{1,0:T(8,128)(2,1)} %all-gather.10.cloned.1.call-done, bf16[512,2048]{1,0:T(8,128)(2,1)} %all-gather.8.cloned.1.call-done, f32[2048]{0:T(1024)S(1)} %copy-done.2, f32[512]{0:T(512)S(1)} %add_rsqrt_fusion.1), kind=kOutput, calls=%fused_computation.19 | convolution fusion | flops 2420113408 | bytes 9185280 | tf_op jit(solution)/shard_map/dot_general | solution.py:21
  123.1 72.6 %all-gather.12.cloned.1.call-done = bf16[2048,1152]{1,0:T(8,128)(2,1)} async-done(((bf16[256,1152]{1,0:T(8,128)(2,1)}), bf16[2048,1152]{1,0:T(8,128)(2,1)}) %all-gather.12.cloned.1.call-update) | async-done | bytes 4718608 | tf_op jit(solution)/shard_map/all_gather | solution.py:19
  195.7 80.9 %all-gather.14.cloned.1.call-done = bf16[1152,2048]{1,0:T(8,128)(2,1)} async-done(((bf16[1152,256]{1,0:T(8,128)(2,1)}), bf16[1152,2048]{1,0:T(8,128)(2,1)}) %all-gather.14.cloned.1.call-update) | async-done | bytes 4718608 | tf_op jit(solution)/shard_map/all_gather | solution.py:28
  276.6 0.0 copy-done
  276.6 12.2 %convolution_convert_fusion.1 = bf16[512,2048]{1,0:T(8,128)(2,1)} fusion(bf16[1152,2048]{1,0:T(8,128)(2,1)} %all-gather.14.cloned.1.call-done, bf16[2048,1152]{1,0:T(8,128)(2,1)} %all-gather.12.cloned.1.call-done, f32[512,1152]{1,0:T(8,128)} %fusion.11, bf16[512,2048]{1,0:T(8,128)(2,1)S(1)} %copy-done, f32[2048]{0:T(1024)S(1)} %copy-done.2, ...), kind=kOutput, calls=%fused_computation.17 | convolution fusion | flops 4840620032 | bytes 16001024 | tf_op jit(solution)/shard_map/dot_general | solution.py:27
  288.7 0.0 all-reduce.2.cloned.1.call-update
  288.8 0.0 all-gather.16.cloned.1.call-start
  288.8 0.5 all-gather.16.cloned.1.call-update
  289.3 0.0 all-gather.18.cloned.1.call-start
  289.4 0.7 all-gather.18.cloned.1.call-update
  290.1 0.0 all-gather.20.cloned.1.call-start
  290.1 0.7 all-gather.20.cloned.1.call-update
  290.8 0.0 copy-start.3
  290.8 0.2 reduce-scatter.2.cloned.1.call-start
  291.1 47.4 %all-reduce.2.cloned.1.call-done = bf16[512,2048]{1,0:T(8,128)(2,1)} async-done(((bf16[512,2048]{1,0:T(8,128)(2,1)}), bf16[512,2048]{1,0:T(8,128)(2,1)}) %all-reduce.2.cloned.1.call-update) | async-done | bytes 2097168 | tf_op jit(solution)/shard_map/psum | solution.py:35
  338.5 4.0 fusion
  342.5 77.4 %all-gather.16.cloned.1.call-done = bf16[2048,1152]{1,0:T(8,128)(2,1)} async-done(((bf16[256,1152]{1,0:T(8,128)(2,1)}), bf16[2048,1152]{1,0:T(8,128)(2,1)}) %all-gather.16.cloned.1.call-update) | async-done | bytes 4718608 | tf_op jit(solution)/shard_map/all_gather | solution.py:18
  419.9 0.0 copy-done.3
  419.9 0.0 copy-start.1
  419.9 7.4 %fusion.15 = f32[512,1152]{1,0:T(8,128)} fusion(bf16[2048,1152]{1,0:T(8,128)(2,1)} %all-gather.16.cloned.1.call-done, bf16[512,2048]{1,0:T(8,128)(2,1)} %get-tuple-element.6, f32[2048]{0:T(1024)S(1)} %copy-done.3, f32[512]{0:T(512)S(1)} %add_rsqrt_fusion), kind=kOutput, calls=%fused_computation.20 | convolution fusion | flops 2420113408 | bytes 9185280 | tf_op jit(solution)/shard_map/dot_general | solution.py:21
  427.4 72.5 %all-gather.18.cloned.1.call-done = bf16[2048,1152]{1,0:T(8,128)(2,1)} async-done(((bf16[256,1152]{1,0:T(8,128)(2,1)}), bf16[2048,1152]{1,0:T(8,128)(2,1)}) %all-gather.18.cloned.1.call-update) | async-done | bytes 4718608 | tf_op jit(solution)/shard_map/all_gather | solution.py:19
  499.8 81.0 %all-gather.20.cloned.1.call-done = bf16[1152,2048]{1,0:T(8,128)(2,1)} async-done(((bf16[1152,256]{1,0:T(8,128)(2,1)}), bf16[1152,2048]{1,0:T(8,128)(2,1)}) %all-gather.20.cloned.1.call-update) | async-done | bytes 4718608 | tf_op jit(solution)/shard_map/all_gather | solution.py:28
  580.9 0.0 copy-done.1
  580.9 12.1 %convolution_convert_fusion = bf16[512,2048]{1,0:T(8,128)(2,1)} fusion(bf16[1152,2048]{1,0:T(8,128)(2,1)} %all-gather.20.cloned.1.call-done, bf16[2048,1152]{1,0:T(8,128)(2,1)} %all-gather.18.cloned.1.call-done, f32[512,1152]{1,0:T(8,128)} %fusion.15, bf16[512,2048]{1,0:T(8,128)(2,1)S(1)} %copy-done.1, f32[2048]{0:T(1024)S(1)} %copy-done.3, ...), kind=kOutput, calls=%fused_computation.16 | convolution fusion | flops 4840620032 | bytes 16001024 | tf_op jit(solution)/shard_map/dot_general | solution.py:27
  593.0 0.0 reduce-scatter.2.cloned.1.call-update
  593.1 29.5 %reduce-scatter.2.cloned.1.call-done = bf16[128,2048]{1,0:T(8,128)(2,1)} async-done(((bf16[512,2048]{1,0:T(8,128)(2,1)}), bf16[128,2048]{1,0:T(8,128)(2,1)}) %reduce-scatter.2.cloned.1.call-update) | async-done | bytes 524304 | tf_op jit(solution)/shard_map/reduce_scatter | solution.py:41
  622.5 2.0 add_convert_fusion
  (2 shorter events, 0.0 us)
Async XLA Ops:
  6.5 109.2 %copy-start.2 = (f32[2048]{0:T(1024)S(1)}, f32[2048]{0:T(1024)}, u32[]{:S(2)}) copy-start(f32[2048]{0:T(1024)} %param.10) | copy-start | bytes 24580
  6.5 27.7 %all-gather.8.cloned.1.call-start = ((), (), s32[]{:S(2)}) async-start(), calls=%async_computation.1 | async-start | bytes 2621440 | tf_op jit(solution)/shard_map/all_gather | solution.py:33
  7.3 108.5 %all-gather.10.cloned.1.call-start = ((), (), s32[]{:S(2)}) async-start(), calls=%async_computation.2 | async-start | bytes 5308416 | tf_op jit(solution)/shard_map/all_gather | solution.py:18
  8.0 187.7 %all-gather.12.cloned.1.call-start = ((), (), s32[]{:S(2)}) async-start(), calls=%async_computation.3 | async-start | bytes 5308416 | tf_op jit(solution)/shard_map/all_gather | solution.py:19
  8.7 267.8 %all-gather.14.cloned.1.call-start = ((), (), s32[]{:S(2)}) async-start(), calls=%async_computation.4 | async-start | bytes 5308416 | tf_op jit(solution)/shard_map/all_gather | solution.py:28
  9.3 329.1 %all-reduce.2.cloned.1.call-start = ((), (), s32[]{:S(2)}) async-start(), calls=%async_computation.5 | async-start | bytes 4194304 | tf_op jit(solution)/shard_map/psum | solution.py:35
  36.3 240.3 %copy-start = (bf16[512,2048]{1,0:T(8,128)(2,1)S(1)}, bf16[512,2048]{1,0:T(8,128)(2,1)}, u32[]{:S(2)}) copy-start(bf16[512,2048]{1,0:T(8,128)(2,1)} %all-gather.8.cloned.1.call-done) | copy-start | bytes 6291460
  288.8 131.2 %all-gather.16.cloned.1.call-start = ((), (), s32[]{:S(2)}) async-start(), calls=%async_computation.6 | async-start | bytes 5308416 | tf_op jit(solution)/shard_map/all_gather | solution.py:18
  289.3 210.5 %all-gather.18.cloned.1.call-start = ((), (), s32[]{:S(2)}) async-start(), calls=%async_computation.7 | async-start | bytes 5308416 | tf_op jit(solution)/shard_map/all_gather | solution.py:19
  290.1 290.8 %all-gather.20.cloned.1.call-start = ((), (), s32[]{:S(2)}) async-start(), calls=%async_computation.8 | async-start | bytes 5308416 | tf_op jit(solution)/shard_map/all_gather | solution.py:28
  290.8 129.1 %copy-start.3 = (f32[2048]{0:T(1024)S(1)}, f32[2048]{0:T(1024)}, u32[]{:S(2)}) copy-start(f32[2048]{0:T(1024)} %param.14) | copy-start | bytes 24580
  290.8 331.7 %reduce-scatter.2.cloned.1.call-start = ((), (), s32[]{:S(2)}) async-start(), calls=%async_computation.9 | async-start | bytes 2621440 | tf_op jit(solution)/shard_map/reduce_scatter | solution.py:41
  419.9 160.9 %copy-start.1 = (bf16[512,2048]{1,0:T(8,128)(2,1)S(1)}, bf16[512,2048]{1,0:T(8,128)(2,1)}, u32[]{:S(2)}) copy-start(bf16[512,2048]{1,0:T(8,128)(2,1)} %get-tuple-element.6) | copy-start | bytes 6291460
Sparse Core Ops, SparseCore 0:
  8.9 25.2 all-gather.7
  36.4 79.3 all-gather.9
  117.9 77.6 all-gather.11
  197.6 78.9 all-gather.13
  288.9 49.5 all-reduce.1
  340.5 79.3 all-gather.15
  422.1 77.6 all-gather.17
  501.9 78.9 all-gather.19
  593.2 29.3 reduce-scatter.1
where the time goes:
time: 631 us
  waiting for transfers between devices  570 us (90%)
  matrix products  39.1 us (6%)
  between operations  13.2 us (2%)
  other arithmetic  8.11 us (1%)
    all_gather x2, waiting for transfers between devices, down_terms(): lax.all_gather(down_w, 'fs', axis=1, tiled=True)  162 us
    all_gather x2, waiting for transfers between devices, hidden_units(): lax.all_gather(gate_w, 'fs', axis=0, tiled=True)  157 us
    all_gather x2, waiting for transfers between devices, hidden_units(): lax.all_gather(up_w, 'fs', axis=0, tiled=True)  145 us
    psum x1, waiting for transfers between devices, on_device(): lax.psum(first_terms.astype(jnp.bfloat16), 'tp').astype(jnp.float32)  47.4 us
    reduce_scatter x1, waiting for transfers between devices, on_device(): lax.psum_scatter(second_terms.astype(jnp.bfloat16), 'tp', scatter_dimensi...  29.5 us
    all_gather x1, waiting for transfers between devices, on_device(): gathered = lax.all_gather(tokens, 'tp', axis=0, tiled=True)  24.8 us
    dot_general x2, matrix products, down_terms(): jnp.dot(hidden, lax.all_gather(down_w, 'fs', axis=1, tiled=True), preferr...  24.3 us
    dot_general x2, matrix products, hidden_units(): gate_sum = jnp.dot(normed, gate_full, preferred_element_type=jnp.float32)  14.7 us
  transfers between devices with their start and end apart: 9, of which 9 were waited for; matrix products, arithmetic and copies ran while one was open for 3% of the time, Pallas kernels for 0%

commit v1 on v0

--- a/solution.py
+++ b/solution.py
@@ -4,6 +4,13 @@
 from jax.sharding import PartitionSpec as P
 
 eps = 1e-06
+
+
+def swapped_in(x, axis, dim):
+    devices = lax.axis_size(axis)
+    shards = jnp.stack([x for _ in range(devices)])
+    shards = lax.all_to_all(shards, axis, split_axis=0, concat_axis=0)
+    return jnp.concatenate(shards, axis=dim)
 
 
 def normalize(rows, gain):
@@ -15,7 +22,7 @@
 def hidden_units(rows, gain, gate_w, up_w):
     normed = normalize(rows, gain)
     gate_full, up_full = (
-        lax.all_gather(gate_w, "fs", axis=0, tiled=True),
+        swapped_in(gate_w, "fs", 0),
         lax.all_gather(up_w, "fs", axis=0, tiled=True),
     )
     gate_sum = jnp.dot(normed, gate_full, preferred_element_type=jnp.float32)

time: 631 us -> 575 us (0.911)
  waiting for transfers between devices: 570 us -> 495 us
  starting transfers between devices: 0.49 us -> 12.5 us
  local copies, waits for them, and re-layouts: 0.02 us -> 6.56 us
    all_to_all x0 -> x2, waiting for transfers between devices: none -> 242 us  [swapped_in(): shards = lax.all_to_all(shards, axis, split_axis=0, concat_axis=0)]
    all_gather x2 -> x0, waiting for transfers between devices: 157 us -> none  [hidden_units(): lax.all_gather(gate_w, 'fs', axis=0, tiled=True)]
    all_gather x2, waiting for transfers between devices: 162 us -> 81.5 us  [down_terms(): lax.all_gather(down_w, 'fs', axis=1, tiled=True)]
    all_gather x2, waiting for transfers between devices: 145 us -> 82.7 us  [hidden_units(): lax.all_gather(up_w, 'fs', axis=0, tiled=True)]
    all_to_all x0 -> x2, starting transfers between devices: none -> 12 us  [swapped_in(): shards = lax.all_to_all(shards, axis, split_axis=0, concat_axis=0)]
    all_gather x1, waiting for transfers between devices: 24.8 us -> 14.2 us  [on_device(): gathered = lax.all_gather(tokens, 'tp', axis=0, tiled=True)]
    another operation x0 -> x2, local copies, waits for them, and re-layouts: none -> 6.53 us  [swapped_in(): shards = jnp.stack([x for _ in range(devices)])]
  transfers between devices with their start and end apart: 9 -> 9, of which waited for: 9 -> 8; matrix products, arithmetic and copies ran while one was open for 3% -> 5% of each run, Pallas kernels for 0% -> 0%
where the time goes in v1:
time: 575 us; the launch traced here: 574 us
  waiting for transfers between devices  495 us (86%)
  matrix products  39.2 us (7%)
  between operations  13.5 us (2%)
  starting transfers between devices  12.5 us (2%)
  other arithmetic  8.1 us (1%)
  local copies, waits for them, and re-layouts  6.56 us (1%)
    all_to_all x2, waiting for transfers between devices, swapped_in(): shards = lax.all_to_all(shards, axis, split_axis=0, concat_axis=0)  242 us
    all_gather x2, waiting for transfers between devices, hidden_units(): lax.all_gather(up_w, 'fs', axis=0, tiled=True)  82.7 us
    all_gather x2, waiting for transfers between devices, down_terms(): lax.all_gather(down_w, 'fs', axis=1, tiled=True)  81.5 us
    psum x1, waiting for transfers between devices, on_device(): lax.psum(first_terms.astype(jnp.bfloat16), 'tp').astype(jnp.float32)  41.1 us
    reduce_scatter x1, waiting for transfers between devices, on_device(): lax.psum_scatter(second_terms.astype(jnp.bfloat16), 'tp', scatter_dimensi...  29.5 us
    dot_general x2, matrix products, down_terms(): jnp.dot(hidden, lax.all_gather(down_w, 'fs', axis=1, tiled=True), preferr...  24.3 us
    dot_general x2, matrix products, hidden_units(): gate_sum = jnp.dot(normed, gate_full, preferred_element_type=jnp.float32)  14.9 us
    all_gather x1, waiting for transfers between devices, on_device(): gathered = lax.all_gather(tokens, 'tp', axis=0, tiled=True)  14.2 us
  transfers between devices with their start and end apart: 9, of which 8 were waited for; matrix products, arithmetic and copies ran while one was open for 5% of the time, Pallas kernels for 0%

profile of v1, /device:TPU:0, one launch (start us, length us, event | category | flops | bytes accessed | tf_op | source)
XLA Modules:
  0.0 574.4 jit_solution(13343769217725946476)
XLA Ops:
  6.5 0.0 all-gather.6.cloned.1.call-start
  6.5 0.7 all-gather.6.cloned.1.call-update
  7.3 0.0 all-gather.10.cloned.1.call-start
  7.3 0.7 all-gather.10.cloned.1.call-update
  8.0 3.8 stack.4
  11.8 0.0 copy-start.3
  11.8 7.4 %all-to-all-start = ((bf16[8,256,1152]{2,1,0:T(8,128)(2,1)}), bf16[8,256,1152]{2,1,0:T(8,128)(2,1)}, u32[]{:S(2)}, u32[]{:S(2)}) async-start(bf16[8,256,1152]{2,1,0:T(8,128)(2,1)} %stack.4), calls=%async_computation | async-start | bytes 9437184 | tf_op jit(solution)/shard_map/all_to_all | solution.py:12
  19.2 0.0 all-gather.8.cloned.1.call-start
  19.3 0.7 all-gather.8.cloned.1.call-update
  20.0 0.0 all-reduce.2.cloned.1.call-start
  20.0 14.2 %all-gather.6.cloned.1.call-done = bf16[512,2048]{1,0:T(8,128)(2,1)} async-done(((bf16[128,2048]{1,0:T(8,128)(2,1)}), bf16[512,2048]{1,0:T(8,128)(2,1)}) %all-gather.6.cloned.1.call-update) | async-done | bytes 2097168 | tf_op jit(solution)/shard_map/all_gather | solution.py:40
  34.2 2.1 fusion.3
  36.3 141.4 %all-to-all-done = bf16[8,256,1152]{2,1,0:T(8,128)(2,1)} async-done(((bf16[8,256,1152]{2,1,0:T(8,128)(2,1)}), bf16[8,256,1152]{2,1,0:T(8,128)(2,1)}, u32[]{:S(2)}, u32[]{:S(2)}) %all-to-all-start) | async-done | bytes 4718624 | tf_op jit(solution)/shard_map/all_to_all | solution.py:12
  177.7 0.0 copy-done.3
  177.7 0.0 copy-start
  177.7 7.4 %fusion.11 = f32[512,1152]{1,0:T(8,128)} fusion(bf16[2048,1152]{1,0:T(8,128)(2,1)} %bitcast, bf16[512,2048]{1,0:T(8,128)(2,1)} %all-gather.6.cloned.1.call-done, f32[2048]{0:T(1024)S(1)} %copy-done.3, f32[512]{0:T(512)S(1)} %add_rsqrt_fusion.1), kind=kOutput, calls=%fused_computation.19 | convolution fusion | flops 2420113408 | bytes 9185280 | tf_op jit(solution)/shard_map/dot_general | solution.py:28
  185.1 0.0 copy-start.2
  185.1 0.0 all-gather.10.cloned.1.call-done
  185.1 76.4 %all-gather.8.cloned.1.call-done = bf16[2048,1152]{1,0:T(8,128)(2,1)} async-done(((bf16[256,1152]{1,0:T(8,128)(2,1)}), bf16[2048,1152]{1,0:T(8,128)(2,1)}) %all-gather.8.cloned.1.call-update) | async-done | bytes 4718608 | tf_op jit(solution)/shard_map/all_gather | solution.py:26
  261.5 0.0 copy-done
  261.5 12.2 %convolution_convert_fusion.1 = bf16[512,2048]{1,0:T(8,128)(2,1)} fusion(bf16[1152,2048]{1,0:T(8,128)(2,1)} %all-gather.10.cloned.1.call-done, bf16[2048,1152]{1,0:T(8,128)(2,1)} %all-gather.8.cloned.1.call-done, f32[512,1152]{1,0:T(8,128)} %fusion.11, bf16[512,2048]{1,0:T(8,128)(2,1)S(1)} %copy-done, f32[2048]{0:T(1024)S(1)} %copy-done.3, ...), kind=kOutput, calls=%fused_computation.17 | convolution fusion | flops 4840620032 | bytes 16001024 | tf_op jit(solution)/shard_map/dot_general | solution.py:34
  273.7 0.0 all-reduce.2.cloned.1.call-update
  273.7 0.0 all-gather.12.cloned.1.call-start
  273.7 0.5 all-gather.12.cloned.1.call-update
  274.3 0.0 copy-done.2
  274.3 2.7 stack.5
  277.0 4.6 all-to-all-start.1
  281.6 0.0 copy-start.4
  281.6 0.0 all-gather.14.cloned.1.call-start
  281.7 0.5 all-gather.14.cloned.1.call-update
  282.2 0.2 reduce-scatter.2.cloned.1.call-start
  282.4 41.1 %all-reduce.2.cloned.1.call-done = bf16[512,2048]{1,0:T(8,128)(2,1)} async-done(((bf16[512,2048]{1,0:T(8,128)(2,1)}), bf16[512,2048]{1,0:T(8,128)(2,1)}) %all-reduce.2.cloned.1.call-update) | async-done | bytes 2097168 | tf_op jit(solution)/shard_map/psum | solution.py:42
  323.6 4.0 fusion
  327.6 101.0 %all-to-all-done.1 = bf16[8,256,1152]{2,1,0:T(8,128)(2,1)} async-done(((bf16[8,256,1152]{2,1,0:T(8,128)(2,1)}), bf16[8,256,1152]{2,1,0:T(8,128)(2,1)}, u32[]{:S(2)}, u32[]{:S(2)}) %all-to-all-start.1) | async-done | bytes 4718624 | tf_op jit(solution)/shard_map/all_to_all | solution.py:12
  428.6 0.0 copy-done.4
  428.6 0.0 copy-start.1
  428.6 7.5 %fusion.15 = f32[512,1152]{1,0:T(8,128)} fusion(bf16[2048,1152]{1,0:T(8,128)(2,1)} %bitcast.1, bf16[512,2048]{1,0:T(8,128)(2,1)} %get-tuple-element.6, f32[2048]{0:T(1024)S(1)} %copy-done.4, f32[512]{0:T(512)S(1)} %add_rsqrt_fusion), kind=kOutput, calls=%fused_computation.20 | convolution fusion | flops 2420113408 | bytes 9185280 | tf_op jit(solution)/shard_map/dot_general | solution.py:28
  436.1 6.3 %all-gather.12.cloned.1.call-done = bf16[2048,1152]{1,0:T(8,128)(2,1)} async-done(((bf16[256,1152]{1,0:T(8,128)(2,1)}), bf16[2048,1152]{1,0:T(8,128)(2,1)}) %all-gather.12.cloned.1.call-update) | async-done | bytes 4718608 | tf_op jit(solution)/shard_map/all_gather | solution.py:26
  442.4 81.5 %all-gather.14.cloned.1.call-done = bf16[1152,2048]{1,0:T(8,128)(2,1)} async-done(((bf16[1152,256]{1,0:T(8,128)(2,1)}), bf16[1152,2048]{1,0:T(8,128)(2,1)}) %all-gather.14.cloned.1.call-update) | async-done | bytes 4718608 | tf_op jit(solution)/shard_map/all_gather | solution.py:35
  523.9 0.0 copy-done.1
  523.9 12.1 %convolution_convert_fusion = bf16[512,2048]{1,0:T(8,128)(2,1)} fusion(bf16[1152,2048]{1,0:T(8,128)(2,1)} %all-gather.14.cloned.1.call-done, bf16[2048,1152]{1,0:T(8,128)(2,1)} %all-gather.12.cloned.1.call-done, f32[512,1152]{1,0:T(8,128)} %fusion.15, bf16[512,2048]{1,0:T(8,128)(2,1)S(1)} %copy-done.1, f32[2048]{0:T(1024)S(1)} %copy-done.4, ...), kind=kOutput, calls=%fused_computation.16 | convolution fusion | flops 4840620032 | bytes 16001024 | tf_op jit(solution)/shard_map/dot_general | solution.py:34
  536.0 0.0 reduce-scatter.2.cloned.1.call-update
  536.1 29.5 %reduce-scatter.2.cloned.1.call-done = bf16[128,2048]{1,0:T(8,128)(2,1)} async-done(((bf16[512,2048]{1,0:T(8,128)(2,1)}), bf16[128,2048]{1,0:T(8,128)(2,1)}) %reduce-scatter.2.cloned.1.call-update) | async-done | bytes 524304 | tf_op jit(solution)/shard_map/reduce_scatter | solution.py:48
  565.5 2.0 add_convert_fusion
  (2 shorter events, 0.0 us)
Async XLA Ops:
  6.5 27.7 %all-gather.6.cloned.1.call-start = ((), (), s32[]{:S(2)}) async-start(), calls=%async_computation.3 | async-start | bytes 2621440 | tf_op jit(solution)/shard_map/all_gather | solution.py:40
  7.3 177.9 %all-gather.10.cloned.1.call-start = ((), (), s32[]{:S(2)}) async-start(), calls=%async_computation.5 | async-start | bytes 5308416 | tf_op jit(solution)/shard_map/all_gather | solution.py:35
  11.8 165.9 %copy-start.3 = (f32[2048]{0:T(1024)S(1)}, f32[2048]{0:T(1024)}, u32[]{:S(2)}) copy-start(f32[2048]{0:T(1024)} %param.10) | copy-start | bytes 24580
  11.8 165.9 %all-to-all-start = ((bf16[8,256,1152]{2,1,0:T(8,128)(2,1)}), bf16[8,256,1152]{2,1,0:T(8,128)(2,1)}, u32[]{:S(2)}, u32[]{:S(2)}) async-start(bf16[8,256,1152]{2,1,0:T(8,128)(2,1)} %stack.4), calls=%async_computation | async-start | bytes 9437184 | tf_op jit(solution)/shard_map/all_to_all | solution.py:12
  19.2 242.2 %all-gather.8.cloned.1.call-start = ((), (), s32[]{:S(2)}) async-start(), calls=%async_computation.4 | async-start | bytes 5308416 | tf_op jit(solution)/shard_map/all_gather | solution.py:26
  20.0 303.6 %all-reduce.2.cloned.1.call-start = ((), (), s32[]{:S(2)}) async-start(), calls=%async_computation.6 | async-start | bytes 4194304 | tf_op jit(solution)/shard_map/psum | solution.py:42
  177.7 83.8 %copy-start = (bf16[512,2048]{1,0:T(8,128)(2,1)S(1)}, bf16[512,2048]{1,0:T(8,128)(2,1)}, u32[]{:S(2)}) copy-start(bf16[512,2048]{1,0:T(8,128)(2,1)} %all-gather.6.cloned.1.call-done) | copy-start | bytes 6291460
  185.1 89.2 %copy-start.2 = (bf16[256,1152]{1,0:T(8,128)(2,1)S(1)}, bf16[256,1152]{1,0:T(8,128)(2,1)}, u32[]{:S(2)}) copy-start(bf16[256,1152]{1,0:T(8,128)(2,1)} %param.15) | copy-start | bytes 1769476
  273.7 168.7 %all-gather.12.cloned.1.call-start = ((), (), s32[]{:S(2)}) async-start(), calls=%async_computation.7 | async-start | bytes 5308416 | tf_op jit(solution)/shard_map/all_gather | solution.py:26
  277.0 151.6 %all-to-all-start.1 = ((bf16[8,256,1152]{2,1,0:T(8,128)(2,1)}), bf16[8,256,1152]{2,1,0:T(8,128)(2,1)}, u32[]{:S(2)}, u32[]{:S(2)}) async-start(bf16[8,256,1152]{2,1,0:T(8,128)(2,1)} %stack.5), calls=%async_computation.1 | async-start | bytes 9437184 | tf_op jit(solution)/shard_map/all_to_all | solution.py:12
  281.6 147.0 %copy-start.4 = (f32[2048]{0:T(1024)S(1)}, f32[2048]{0:T(1024)}, u32[]{:S(2)}) copy-start(f32[2048]{0:T(1024)} %param.14) | copy-start | bytes 24580
  281.6 242.3 %all-gather.14.cloned.1.call-start = ((), (), s32[]{:S(2)}) async-start(), calls=%async_computation.8 | async-start | bytes 5308416 | tf_op jit(solution)/shard_map/all_gather | solution.py:35
  282.2 283.3 %reduce-scatter.2.cloned.1.call-start = ((), (), s32[]{:S(2)}) async-start(), calls=%async_computation.9 | async-start | bytes 2621440 | tf_op jit(solution)/shard_map/reduce_scatter | solution.py:48
  428.6 95.3 %copy-start.1 = (bf16[512,2048]{1,0:T(8,128)(2,1)S(1)}, bf16[512,2048]{1,0:T(8,128)(2,1)}, u32[]{:S(2)}) copy-start(bf16[512,2048]{1,0:T(8,128)(2,1)} %get-tuple-element.6) | copy-start | bytes 6291460
Sparse Core Ops, SparseCore 0:
  8.9 25.2 all-gather.5
  36.2 144.6 all-gather.9
  183.2 78.2 all-gather.7
  273.8 49.7 all-reduce.1
  325.6 116.7 all-gather.11
  444.3 79.5 all-gather.13
  536.2 29.3 reduce-scatter.1
